TPU v7x, 32 devices: a whole 2x2x4 slice. The times are simulated.
32 devices in a mesh: dp: 4 (over y, x), kv: 4 (over z), tp: 2 (over core).
Axes of the slice: x: 2, y: 2, z: 4, core: 2. Of those that a mesh axis runs over, the one named last changes fastest.
Arguments:
- resid: bfloat16 [16, 2048], P('dp', ('kv', 'tp')), may hold values from -45 to 45
- norm_gain: bfloat16 [3, 2048], P(None, ('kv', 'tp')), may hold values from 0.099609375 to 1.8984375
- ffn_gate: bfloat16 [2, 2048, 5632], P(None, None, ('kv', 'tp')), may hold values from -0.125 to 0.125
- ffn_up: bfloat16 [2, 2048, 5632], P(None, None, ('kv', 'tp')), may hold values from -0.125 to 0.125
- ffn_down: bfloat16 [2, 5632, 2048], P(None, ('kv', 'tp')), may hold values from -0.109375 to 0.109375
- w_x: bfloat16 [2048, 64, 64], P(None, 'kv', 'tp'), may hold values from -0.125 to 0.125
- w_z: bfloat16 [2048, 64, 64], P(None, 'kv', 'tp'), may hold values from -0.125 to 0.125
- w_bc: bfloat16 [2048, 2, 8, 128], P('kv'), may hold values from -0.125 to 0.125
- w_dt: bfloat16 [2048, 64], P('kv'), may hold values from -0.125 to 0.125
- dt_bias: float32 [64], replicated, may hold values from -2 to 0.5
- a_log: float32 [64], replicated, may hold values from -1.5 to 1.5
- d_skip: float32 [64], replicated, may hold values from 0.5 to 1.5
- conv_wx: bfloat16 [4, 64, 64], P(None, None, 'tp'), may hold values from -3 to 3
- conv_wbc: bfloat16 [4, 2, 8, 128], replicated, may hold values from -3 to 3
- conv_x: bfloat16 [16, 3, 64, 64], P(('dp', 'kv'), None, None, 'tp'), may hold values from -6 to 6
- conv_bc: bfloat16 [16, 3, 2, 8, 128], P(('dp', 'kv')), may hold values from -6 to 6
- ssm_state: float32 [16, 64, 64, 128], P(('dp', 'kv'), None, 'tp'), may hold values from -3 to 3
- w_out: bfloat16 [64, 64, 2048], P(None, 'tp', 'kv'), may hold values from -0.09375 to 0.09375
Outputs:
- final: bfloat16 [16, 2048], P('dp', ('kv', 'tp'))
All inputs are finite; a program needn't handle non-finite values.
Results may differ from a plain program's by a relative error of at most 0.018.
Values may be sent and summed in bfloat16 or wider, within the bound.
No kernel may reach another device: no remote copies, remote signals or barrier semaphores. Data moves between devices by JAX's collectives and lax.ppermute only.
A program may use at most 64 MiB of HBM per device.

v0:
```python
import jax
import jax.numpy as jnp
from jax import lax
from jax.sharding import PartitionSpec as P

D = 2048
EPS = 1e-06


def normalize(rows, gain):
    values = rows.astype(jnp.float32)
    scale = lax.rsqrt(jnp.mean(values * values, axis=1, keepdims=True) + EPS)
    return (values * scale * gain.astype(jnp.float32).reshape(1, -1)).astype(jnp.bfloat16)


def feed_forward(normed, w_gate, w_up, w_down):
    gate = jnp.dot(normed, w_gate, preferred_element_type=jnp.float32)
    upper = jnp.dot(normed, w_up, preferred_element_type=jnp.float32)
    hidden = (jax.nn.silu(gate) * upper).astype(jnp.bfloat16)
    return jnp.dot(hidden, w_down, preferred_element_type=jnp.float32)


def add_half(base, sums):
    return (base.astype(jnp.float32) + 0.5 * sums).astype(jnp.bfloat16)


def ffn_totals(partial_value):
    return lax.psum(partial_value, ("kv", "tp"))


def short_conv(history, newest, taps):
    window = jnp.concatenate(
        [history.astype(jnp.float32), newest.astype(jnp.float32)[:, None]], axis=1
    )
    return jax.nn.silu(jnp.sum(window * taps.astype(jnp.float32)[None], axis=1))


def state_step(
    xs_new,
    zeta,
    bc_new,
    dt_raw,
    conv_x,
    conv_bc,
    ssm_state,
    conv_wx,
    conv_wbc,
    dt_bias,
    a_log,
    d_skip,
):
    xconv = short_conv(conv_x, xs_new, conv_wx)
    bconv = short_conv(conv_bc, bc_new, conv_wbc)
    heads = xconv.shape[1]
    groups = bconv.shape[2]
    bmat = jnp.repeat(bconv[:, 0], heads // groups, axis=1)
    cmat = jnp.repeat(bconv[:, 1], heads // groups, axis=1)
    step_size = jax.nn.softplus(dt_raw + dt_bias[None, :])
    decay = jnp.exp(-step_size * jnp.exp(a_log)[None, :])
    updated = (
        decay[:, :, None, None] * ssm_state
        + (step_size[:, :, None] * xconv)[..., None] * bmat[:, :, None, :]
    )
    mixed = (
        jnp.einsum("shpn,shn->shp", updated, cmat, precision=lax.Precision.HIGHEST)
        + d_skip[None, :, None] * xconv
    )
    return (mixed * jax.nn.silu(zeta.astype(jnp.float32))).astype(jnp.bfloat16)


def group_terms(slab, w_bc, w_dt):
    span = slab.shape[1]
    flat_bc = w_bc.reshape(span, -1)
    bc_part = jnp.dot(slab, flat_bc, preferred_element_type=jnp.float32)
    dt_part = jnp.dot(slab, w_dt, preferred_element_type=jnp.float32)
    return (
        lax.psum_scatter(bc_part, "kv", scatter_dimension=0, tiled=True),
        lax.psum_scatter(dt_part, "kv", scatter_dimension=0, tiled=True),
    )


def mix_partial(
    normed,
    w_x,
    w_z,
    w_bc,
    w_dt,
    dt_bias,
    a_log,
    d_skip,
    conv_wx,
    conv_wbc,
    conv_x,
    conv_bc,
    ssm_state,
    w_out,
):
    rows = normed.shape[0]
    local_heads = w_x.shape[1]
    half = w_x.shape[2]
    xs_part = (
        jnp.dot(normed, w_x.reshape(D, -1), preferred_element_type=jnp.float32)
        .astype(jnp.bfloat16)
        .reshape(rows, local_heads, half)
    )
    zeta_part = (
        jnp.dot(normed, w_z.reshape(D, -1), preferred_element_type=jnp.float32)
        .astype(jnp.bfloat16)
        .reshape(rows, local_heads, half)
    )
    xs_new, zeta = (
        lax.all_to_all(xs_part, "kv", split_axis=0, concat_axis=1, tiled=True),
        lax.all_to_all(zeta_part, "kv", split_axis=0, concat_axis=1, tiled=True),
    )
    span = w_bc.shape[0]
    slab = lax.dynamic_slice_in_dim(normed, lax.axis_index("kv") * span, span, 1)
    bc_sum, dt_raw = group_terms(slab, w_bc, w_dt)
    bc_new = bc_sum.astype(jnp.bfloat16).reshape((bc_sum.shape[0],) + w_bc.shape[1:])
    mixed = state_step(
        xs_new,
        zeta,
        bc_new,
        dt_raw,
        conv_x,
        conv_bc,
        ssm_state,
        conv_wx,
        conv_wbc,
        dt_bias,
        a_log,
        d_skip,
    )
    flat_out = w_out.reshape(-1, w_out.shape[2])
    piece = lax.all_gather(mixed, "kv", axis=0, tiled=True)
    return jnp.dot(piece.reshape(piece.shape[0], -1), flat_out, preferred_element_type=jnp.float32)


def per_device(
    resid,
    norm_gain,
    ffn_gate,
    ffn_up,
    ffn_down,
    w_x,
    w_z,
    w_bc,
    w_dt,
    dt_bias,
    a_log,
    d_skip,
    conv_wx,
    conv_wbc,
    conv_x,
    conv_bc,
    ssm_state,
    w_out,
):
    mixer_args = (
        w_x,
        w_z,
        w_bc,
        w_dt,
        dt_bias,
        a_log,
        d_skip,
        conv_wx,
        conv_wbc,
        conv_x,
        conv_bc,
        ssm_state,
        w_out,
    )
    rows, gains = (
        lax.all_gather(resid, ("kv", "tp"), axis=1, tiled=True),
        lax.all_gather(norm_gain, ("kv", "tp"), axis=1, tiled=True),
    )
    first = add_half(
        rows,
        ffn_totals(feed_forward(normalize(rows, gains[0]), ffn_gate[0], ffn_up[0], ffn_down[0])),
    )
    partial_value = mix_partial(normalize(first, gains[1]), *mixer_args)
    span = partial_value.shape[1]
    block = lax.dynamic_slice_in_dim(first, lax.axis_index("kv") * span, span, 1)
    joined = (block.astype(jnp.float32) + lax.psum(partial_value, "tp")).astype(jnp.bfloat16)
    second = lax.all_gather(joined, "kv", axis=1, tiled=True)
    final = add_half(
        second,
        ffn_totals(feed_forward(normalize(second, gains[2]), ffn_gate[1], ffn_up[1], ffn_down[1])),
    )
    width = resid.shape[1]
    return lax.dynamic_slice_in_dim(final, lax.axis_index(("kv", "tp")) * width, width, 1)


def solution(mesh):
    placed = (
        P("dp", ("kv", "tp")),
        P(None, ("kv", "tp")),
        P(None, None, ("kv", "tp")),
        P(None, None, ("kv", "tp")),
        P(None, ("kv", "tp"), None),
        P(None, "kv", "tp"),
        P(None, "kv", "tp"),
        P("kv", None, None, None),
        P("kv", None),
        P(),
        P(),
        P(),
        P(None, None, "tp"),
        P(),
        P(("dp", "kv"), None, None, "tp"),
        P(("dp", "kv"), None, None, None, None),
        P(("dp", "kv"), None, "tp", None),
        P(None, "tp", "kv"),
    )
    return jax.shard_map(
        per_device, mesh=mesh, in_specs=placed, out_specs=P("dp", ("kv", "tp")), check_vma=False
    )
```

profile of v0, /device:TPU:0, one launch (start us, length us, event | category | flops | bytes accessed | tf_op | source)
XLA Modules:
  0.0 168.5 jit_solution(16530086735748407296)
XLA Ops:
  0.0 14.7 %all_gather.12 = bf16[4,2048]{1,0:T(4,128)(2,1)S(1)} all-gather(bf16[4,256]{1,0:T(4,128)(2,1)} %param.18), channel_id=1, replica_groups=mesh['dp'=4,'kv'=4,'tp'=2] {'kv','tp'}, dimensions={1}, use_global_device_ids=true | all-gather | bytes 18432 | tf_op jit(solution)/shard_map/all_gather | solution.py:174
  14.9 12.9 %all_gather.13 = bf16[3,2048]{1,0:T(4,128)(2,1)S(1)} all-gather(bf16[3,256]{1,0:T(4,128)(2,1)} %param.19), channel_id=1, replica_groups=mesh['dp'=4,'kv'=4,'tp'=2] {'kv','tp'}, dimensions={1}, use_global_device_ids=true | all-gather | bytes 13824 | tf_op jit(solution)/shard_map/all_gather | solution.py:175
  27.8 2.7 %fusion.10 = f32[4,704]{1,0:T(4,128)S(1)} fusion(bf16[2,2048,704]{1,2,0:T(8,128)(2,1)} %param.20, bf16[4,2048]{1,0:T(4,128)(2,1)S(1)} %all_gather.12, f32[2048]{0:T(1024)S(1)} %bitcast.113, f32[4]{0:T(128)S(1)} %add_rsqrt_fusion.2), kind=kOutput, calls=%fused_computation.10 | convolution fusion | flops 11567104 | bytes 2919440 | tf_op jit(solution)/shard_map/dot_general | solution.py:17
  30.5 4.4 %fusion.6 = f32[4,2048]{1,0:T(4,128)S(1)} fusion(bf16[2,704,2048]{2,1,0:T(8,128)(2,1)} %param.22, bf16[2,2048,704]{1,2,0:T(8,128)(2,1)} %param.21, f32[4,704]{1,0:T(4,128)S(1)} %fusion.10, bf16[4,2048]{1,0:T(4,128)(2,1)S(1)} %all_gather.12, f32[2048]{0:T(1024)S(1)} %bitcast.114, f32[4]{0:T(128)S(1)} %add_rsqrt_fusion.2), kind=kOutput, calls=%fused_computation.6 | convolution fusion | flops 23118336 | bytes 5835792 | tf_op jit(solution)/shard_map/dot_general | solution.py:20
  34.8 26.7 %psum.21 = f32[4,2048]{1,0:T(4,128)S(1)} all-reduce(f32[4,2048]{1,0:T(4,128)S(1)} %fusion.6), channel_id=1, replica_groups=mesh['dp'=4,'kv'=4,'tp'=2] {'kv','tp'}, use_global_device_ids=true, to_apply=%region_1.2 | all-reduce | flops 8192 | bytes 65536 | tf_op jit(solution)/shard_map/psum | solution.py:28
  61.8 0.6 convolution_convert_fusion.1
  62.5 0.7 reshape.219
  63.2 3.2 %all-to-all-start = ((bf16[4,2,256]{2,1,0:T(2,128)(2,1)}), bf16[4,2,256]{2,1,0:T(2,128)(2,1)S(1)}, u32[]{:S(2)}, u32[]{:S(2)}) async-start(bf16[4,2,256]{2,1,0:T(2,128)(2,1)} %reshape.219), calls=%async_computation | async-start | bytes 8192 | tf_op jit(solution)/shard_map/all_to_all | solution.py:112
  66.5 2.2 %convolution_convert_fusion = bf16[4,512]{1,0:T(4,128)(2,1)S(1)} fusion(bf16[4,2048]{1,0:T(4,128)(2,1)S(1)} %fusion.47, bf16[2048,512]{0,1:T(8,128)(2,1)} %bitcast.109), kind=kOutput, calls=%fused_computation.26 | convolution fusion | flops 8390656 | bytes 2117632 | tf_op jit(solution)/shard_map/dot_general | solution.py:107
  68.9 2.0 %fusion.18 = f32[4,2048]{1,0:T(4,128)S(1)} fusion(bf16[64,8,16,128]{3,2,1,0:T(8,128)(2,1)} %bitcast.108, bf16[4,2048]{1,0:T(4,128)(2,1)S(1)} %fusion.47, s32[]{:T(128)S(6)} %select_n.11), kind=kOutput, calls=%fused_computation.18 | convolution fusion | flops 8388608 | bytes 2134020 | tf_op jit(solution)/shard_map/dot_general | solution.py:74
  71.4 19.8 %all-reduce.2 = (bf16[4,2048]{1,0:T(4,128)(2,1)S(1)}, f32[4,64]{1,0:T(4,128)S(1)}) all-reduce(f32[4,2048]{1,0:T(4,128)S(1)} %fusion.18, f32[4,64]{1,0:T(4,128)S(1)} %fusion.69), channel_id=4, replica_groups=mesh['dp'=4,'kv'=4,'tp'=2] {'kv'}, use_global_device_ids=true, to_apply=%region_5.6.clone | all-reduce | flops 8448 | bytes 51200
  91.2 0.7 fusion.60
  92.1 0.7 reshape.217
  92.8 3.2 %all-to-all-start.1 = ((bf16[4,2,256]{2,1,0:T(2,128)(2,1)}), bf16[4,2,256]{2,1,0:T(2,128)(2,1)S(1)}, u32[]{:S(2)}, u32[]{:S(2)}) async-start(bf16[4,2,256]{2,1,0:T(2,128)(2,1)} %reshape.217), calls=%async_computation.1 | async-start | bytes 8192 | tf_op jit(solution)/shard_map/all_to_all | solution.py:113
  96.0 0.7 fusion.75
  96.9 4.7 %all-to-all-done.1 = bf16[4,2,256]{2,1,0:T(2,128)(2,1)S(1)} async-done(((bf16[4,2,256]{2,1,0:T(2,128)(2,1)}), bf16[4,2,256]{2,1,0:T(2,128)(2,1)S(1)}, u32[]{:S(2)}, u32[]{:S(2)}) %all-to-all-start.1) | async-done | bytes 4128 | tf_op jit(solution)/shard_map/all_to_all | solution.py:113
  101.9 1.9 %fusion.33 = f32[64,1,32]{2,1,0:T(1,128)S(1)} fusion(f32[64,128,1]{1,2,0:T(1,128)S(1)} %bitcast.110, f32[1,64,32,128]{3,2,1,0:T(8,128)S(1)} %copy-done.1, f32[64,128]{1,0:T(8,128)S(1)} %broadcast_bitcast_fusion, f32[64,32]{1,0:T(8,128)S(1)} %copy.28, f32[64]{0:T(128)S(1)} %get-tuple-element.7), kind=kOutput, calls=%fused_computation.28 | convolution fusion | flops 3932160 | bytes 1130752 | tf_op jit(solution)/shard_map/shpn,shn->shp/dot_general | solution.py:65
  103.9 13.1 %all-gather.1 = bf16[4,64,32]{1,2,0:T(8,128)(2,1)S(1)} all-gather(bf16[1,64,32]{1,2,0:T(8,128)(2,1)S(1)} %fusion.64), channel_id=2, replica_groups=mesh['dp'=4,'kv'=4,'tp'=2] {'kv'}, dimensions={0}, use_global_device_ids=true | all-gather | bytes 20480 | tf_op jit(solution)/shard_map/all_gather | solution.py:134
  117.1 2.0 %convolution_bitcast_fusion = f32[4,512]{1,0:T(4,128)S(1)} fusion(bf16[4,64,32]{2,0,1:T(4,128)(2,1)S(1)} %copy.35, bf16[64,32,512]{2,1,0:T(8,128)(2,1)} %param.35), kind=kOutput, calls=%fused_computation.25 | convolution fusion | flops 8388608 | bytes 2121728 | tf_op jit(solution)/shard_map/dot_general | solution.py:135
  119.2 2.5 %psum.22 = f32[4,512]{1,0:T(4,128)S(1)} all-reduce(f32[4,512]{1,0:T(4,128)S(1)} %convolution_bitcast_fusion), channel_id=1, replica_groups=mesh['dp'=4,'kv'=4,'tp'=2] {'tp'}, use_global_device_ids=true, to_apply=%region_7.8 | all-reduce | flops 2048 | bytes 16384 | tf_op jit(solution)/shard_map/psum | solution.py:184
  121.6 13.2 %all_gather.15 = bf16[4,2048]{1,0:T(4,128)(2,1)S(1)} all-gather(bf16[4,512]{1,0:T(4,128)(2,1)S(1)} %add_convert_fusion), channel_id=1, replica_groups=mesh['dp'=4,'kv'=4,'tp'=2] {'kv'}, dimensions={1}, use_global_device_ids=true | all-gather | bytes 20480 | tf_op jit(solution)/shard_map/all_gather | solution.py:185
  135.0 2.7 %fusion.4 = f32[4,704]{1,0:T(4,128)S(1)} fusion(bf16[2,2048,704]{1,2,0:T(8,128)(2,1)} %param.20, f32[2048]{0:T(1024)S(1)} %bitcast.111, f32[4]{0:T(128)S(1)} %add_rsqrt_fusion, bf16[4,2048]{1,0:T(4,128)(2,1)S(1)} %all_gather.15), kind=kOutput, calls=%fused_computation.4 | convolution fusion | flops 11567104 | bytes 2919440 | tf_op jit(solution)/shard_map/dot_general | solution.py:17
  137.7 4.4 %fusion = f32[4,2048]{1,0:T(4,128)S(1)} fusion(bf16[2,704,2048]{2,1,0:T(8,128)(2,1)} %param.22, bf16[2,2048,704]{1,2,0:T(8,128)(2,1)} %param.21, f32[4,704]{1,0:T(4,128)S(1)} %fusion.4, f32[2048]{0:T(1024)S(1)} %bitcast.112, f32[4]{0:T(128)S(1)} %add_rsqrt_fusion, bf16[4,2048]{1,0:T(4,128)(2,1)S(1)} %all_gather.15), kind=kOutput, calls=%fused_computation | convolution fusion | flops 23118336 | bytes 5835792 | tf_op jit(solution)/shard_map/dot_general | solution.py:20
  142.0 25.9 %psum.23 = f32[4,2048]{1,0:T(4,128)S(1)} all-reduce(f32[4,2048]{1,0:T(4,128)S(1)} %fusion), channel_id=1, replica_groups=mesh['dp'=4,'kv'=4,'tp'=2] {'kv','tp'}, use_global_device_ids=true, to_apply=%region_9.10 | all-reduce | flops 8192 | bytes 65536 | tf_op jit(solution)/shard_map/psum | solution.py:28
  (54 shorter events, 2.8 us)
Async XLA Ops:
  0.0 61.7 %copy-start = (bf16[2048,16,32]{0,2,1:T(8,128)(2,1)S(1)}, bf16[2048,16,32]{0,2,1:T(8,128)(2,1)}, u32[]{:S(2)}) copy-start(bf16[2048,16,32]{0,2,1:T(8,128)(2,1)} %param.23) | copy-start | bytes 6291460
  34.8 33.9 %copy-start.2 = (bf16[512,64]{0,1:T(8,128)(2,1)S(1)}, bf16[512,64]{0,1:T(8,128)(2,1)}, u32[]{:S(2)}) copy-start(bf16[512,64]{0,1:T(8,128)(2,1)} %param.26) | copy-start | bytes 196612
  61.7 9.1 %copy-start.10 = (u32[32]{0:T(128)S(1)}, u32[32]{0:T(128)}, u32[]{:S(2)}) copy-start(u32[32]{0:T(128)} %constant.45) | copy-start | bytes 388
  61.7 30.2 %copy-start.5 = (bf16[4,2,8,128]{3,2,1,0:T(8,128)(2,1)S(1)}, bf16[4,2,8,128]{3,2,1,0:T(8,128)(2,1)}, u32[]{:S(2)}) copy-start(bf16[4,2,8,128]{3,2,1,0:T(8,128)(2,1)} %param.31) | copy-start | bytes 49156
  61.8 30.2 %copy-start.6 = (bf16[1,3,2,8,128]{4,3,2,1,0:T(8,128)(2,1)S(1)}, bf16[1,3,2,8,128]{4,3,2,1,0:T(8,128)(2,1)}, u32[]{:S(2)}) copy-start(bf16[1,3,2,8,128]{4,3,2,1,0:T(8,128)(2,1)} %param.33) | copy-start | bytes 36868
  61.8 34.2 %copy-start.8 = (f32[64]{0:T(128)S(1)}, f32[64]{0:T(128)}, u32[]{:S(2)}) copy-start(f32[64]{0:T(128)} %param.28) | copy-start | bytes 772
  61.8 34.2 %copy-start.9 = (f32[64]{0:T(128)S(1)}, f32[64]{0:T(128)}, u32[]{:S(2)}) copy-start(f32[64]{0:T(128)} %param.27) | copy-start | bytes 772
  62.4 39.3 %copy-start.3 = (bf16[4,64,32]{1,2,0:T(8,128)(2,1)S(1)}, bf16[4,64,32]{1,2,0:T(8,128)(2,1)}, u32[]{:S(2)}) copy-start(bf16[4,64,32]{1,2,0:T(8,128)(2,1)} %param.30) | copy-start | bytes 49156
  62.4 39.3 %copy-start.4 = (bf16[1,3,64,32]{2,3,1,0:T(8,128)(2,1)S(1)}, bf16[1,3,64,32]{2,3,1,0:T(8,128)(2,1)}, u32[]{:S(2)}) copy-start(bf16[1,3,64,32]{2,3,1,0:T(8,128)(2,1)} %param.32) | copy-start | bytes 36868
  62.4 39.4 %copy-start.1 = (f32[1,64,32,128]{3,2,1,0:T(8,128)S(1)}, f32[1,64,32,128]{3,2,1,0:T(8,128)}, u32[]{:S(2)}) copy-start(f32[1,64,32,128]{3,2,1,0:T(8,128)} %param.34) | copy-start | bytes 3145732
  63.2 29.5 %all-to-all-start = ((bf16[4,2,256]{2,1,0:T(2,128)(2,1)}), bf16[4,2,256]{2,1,0:T(2,128)(2,1)S(1)}, u32[]{:S(2)}, u32[]{:S(2)}) async-start(bf16[4,2,256]{2,1,0:T(2,128)(2,1)} %reshape.219), calls=%async_computation | async-start | bytes 8192 | tf_op jit(solution)/shard_map/all_to_all | solution.py:112
  66.5 37.4 %copy-start.7 = (f32[64]{0:T(128)S(1)}, f32[64]{0:T(128)}, u32[]{:S(2)}) copy-start(f32[64]{0:T(128)} %param.29) | copy-start | bytes 772
  92.8 8.8 %all-to-all-start.1 = ((bf16[4,2,256]{2,1,0:T(2,128)(2,1)}), bf16[4,2,256]{2,1,0:T(2,128)(2,1)S(1)}, u32[]{:S(2)}, u32[]{:S(2)}) async-start(bf16[4,2,256]{2,1,0:T(2,128)(2,1)} %reshape.217), calls=%async_computation.1 | async-start | bytes 8192 | tf_op jit(solution)/shard_map/all_to_all | solution.py:113
where the time goes:
time: 169 us
  blocking collectives  129 us (76%)
  matrix products  22.9 us (14%)
  starting transfers between devices  6.47 us (4%)
  waiting for transfers between devices  4.68 us (3%)
  local copies, waits for them, and re-layouts  3.47 us (2%)
  other arithmetic  1.89 us (1%)
    psum x2, blocking collectives, ffn_totals(): return lax.psum(partial_value, ('kv', 'tp'))  52.6 us
    unnamed x1, blocking collectives  19.8 us
    all_gather x1, blocking collectives, per_device(): lax.all_gather(resid, ('kv', 'tp'), axis=1, tiled=True)  14.7 us
    all_gather x1, blocking collectives, per_device(): second = lax.all_gather(joined, 'kv', axis=1, tiled=True)  13.2 us
    all_gather x1, blocking collectives, mix_partial(): piece = lax.all_gather(mixed, 'kv', axis=0, tiled=True)  13.1 us
    all_gather x1, blocking collectives, per_device(): lax.all_gather(norm_gain, ('kv', 'tp'), axis=1, tiled=True)  12.9 us
    dot_general x2, matrix products, feed_forward(): return jnp.dot(hidden, w_down, preferred_element_type=jnp.float32)  8.72 us
    dot_general x2, matrix products, feed_forward(): gate = jnp.dot(normed, w_gate, preferred_element_type=jnp.float32)  5.31 us
  transfers between devices with their start and end apart: 2, of which 1 were waited for; matrix products, arithmetic and copies ran while one was open for 4% of the time, Pallas kernels for 0%

commit v1 on v0

--- a/solution.py
+++ b/solution.py
@@ -5,6 +5,12 @@
 
 D = 2048
 EPS = 1e-06
+
+
+def match_matrix(original):
+    for dev in ("tp", "kv"):
+        original = jax.lax.psum(original, dev)
+    return original
 
 
 def normalize(rows, gain):
@@ -25,7 +31,7 @@
 
 
 def ffn_totals(partial_value):
-    return lax.psum(partial_value, ("kv", "tp"))
+    return match_matrix(partial_value)
 
 
 def short_conv(history, newest, taps):

time: 169 us -> 156 us (0.923)
  blocking collectives: 129 us -> 116 us
    psum x2 -> x4, blocking collectives: 52.6 us -> 39.8 us  [match_matrix(): original = jax.lax.psum(original, dev)]
  transfers between devices with their start and end apart: 2 -> 2, of which waited for: 1 -> 1; matrix products, arithmetic and copies ran while one was open for 4% -> 5% of each run, Pallas kernels for 0% -> 0%
where the time goes in v1:
time: 156 us
  blocking collectives  116 us (74%)
  matrix products  22.9 us (15%)
  starting transfers between devices  6.47 us (4%)
  waiting for transfers between devices  4.68 us (3%)
  local copies, waits for them, and re-layouts  3.47 us (2%)
  other arithmetic  1.9 us (1%)
    psum x4, blocking collectives, match_matrix(): original = jax.lax.psum(original, dev)  39.8 us
    unnamed x1, blocking collectives  19.8 us
    all_gather x1, blocking collectives, per_device(): lax.all_gather(resid, ('kv', 'tp'), axis=1, tiled=True)  14.7 us
    all_gather x1, blocking collectives, per_device(): second = lax.all_gather(joined, 'kv', axis=1, tiled=True)  13.2 us
    all_gather x1, blocking collectives, mix_partial(): piece = lax.all_gather(mixed, 'kv', axis=0, tiled=True)  13.1 us
    all_gather x1, blocking collectives, per_device(): lax.all_gather(norm_gain, ('kv', 'tp'), axis=1, tiled=True)  12.9 us
    dot_general x2, matrix products, feed_forward(): return jnp.dot(hidden, w_down, preferred_element_type=jnp.float32)  8.72 us
    dot_general x2, matrix products, feed_forward(): gate = jnp.dot(normed, w_gate, preferred_element_type=jnp.float32)  5.31 us
  transfers between devices with their start and end apart: 2, of which 1 were waited for; matrix products, arithmetic and copies ran while one was open for 5% of the time, Pallas kernels for 0%

profile of v1, /device:TPU:0, one launch (start us, length us, event | category | flops | bytes accessed | tf_op | source)
XLA Modules:
  0.0 155.9 jit_solution(8590855458713456822)
XLA Ops:
  0.0 14.7 %all_gather.12 = bf16[4,2048]{1,0:T(4,128)(2,1)S(1)} all-gather(bf16[4,256]{1,0:T(4,128)(2,1)} %param.18), channel_id=1, replica_groups=mesh['dp'=4,'kv'=4,'tp'=2] {'kv','tp'}, dimensions={1}, use_global_device_ids=true | all-gather | bytes 18432 | tf_op jit(solution)/shard_map/all_gather | solution.py:180
  14.9 12.9 %all_gather.13 = bf16[3,2048]{1,0:T(4,128)(2,1)S(1)} all-gather(bf16[3,256]{1,0:T(4,128)(2,1)} %param.19), channel_id=1, replica_groups=mesh['dp'=4,'kv'=4,'tp'=2] {'kv','tp'}, dimensions={1}, use_global_device_ids=true | all-gather | bytes 13824 | tf_op jit(solution)/shard_map/all_gather | solution.py:181
  27.8 2.7 %fusion.10 = f32[4,704]{1,0:T(4,128)S(1)} fusion(bf16[2,2048,704]{1,2,0:T(8,128)(2,1)} %param.20, bf16[4,2048]{1,0:T(4,128)(2,1)S(1)} %all_gather.12, f32[2048]{0:T(1024)S(1)} %bitcast.113, f32[4]{0:T(128)S(1)} %add_rsqrt_fusion.2), kind=kOutput, calls=%fused_computation.10 | convolution fusion | flops 11567104 | bytes 2919440 | tf_op jit(solution)/shard_map/dot_general | solution.py:23
  30.5 4.4 %fusion.6 = f32[4,2048]{1,0:T(4,128)S(1)} fusion(bf16[2,704,2048]{2,1,0:T(8,128)(2,1)} %param.22, bf16[2,2048,704]{1,2,0:T(8,128)(2,1)} %param.21, f32[4,704]{1,0:T(4,128)S(1)} %fusion.10, bf16[4,2048]{1,0:T(4,128)(2,1)S(1)} %all_gather.12, f32[2048]{0:T(1024)S(1)} %bitcast.114, f32[4]{0:T(128)S(1)} %add_rsqrt_fusion.2), kind=kOutput, calls=%fused_computation.6 | convolution fusion | flops 23118336 | bytes 5835792 | tf_op jit(solution)/shard_map/dot_general | solution.py:26
  34.8 3.7 %psum.35 = f32[4,2048]{1,0:T(4,128)S(1)} all-reduce(f32[4,2048]{1,0:T(4,128)S(1)} %fusion.6), channel_id=1, replica_groups=mesh['dp'=4,'kv'=4,'tp'=2] {'tp'}, use_global_device_ids=true, to_apply=%region_1.2 | all-reduce | flops 8192 | bytes 65536 | tf_op jit(solution)/shard_map/psum | solution.py:12
  38.5 16.5 %psum.36 = f32[4,2048]{1,0:T(4,128)S(1)} all-reduce(f32[4,2048]{1,0:T(4,128)S(1)} %psum.35), channel_id=1, replica_groups=mesh['dp'=4,'kv'=4,'tp'=2] {'kv'}, use_global_device_ids=true, to_apply=%region_2.3 | all-reduce | flops 8192 | bytes 65536 | tf_op jit(solution)/shard_map/psum | solution.py:12
  56.1 0.7 reshape.219
  56.7 3.2 %all-to-all-start = ((bf16[4,2,256]{2,1,0:T(2,128)(2,1)}), bf16[4,2,256]{2,1,0:T(2,128)(2,1)S(1)}, u32[]{:S(2)}, u32[]{:S(2)}) async-start(bf16[4,2,256]{2,1,0:T(2,128)(2,1)} %reshape.219), calls=%async_computation | async-start | bytes 8192 | tf_op jit(solution)/shard_map/all_to_all | solution.py:118
  60.0 2.2 %convolution_convert_fusion = bf16[4,512]{1,0:T(4,128)(2,1)S(1)} fusion(bf16[4,2048]{1,0:T(4,128)(2,1)S(1)} %fusion.47, bf16[2048,512]{0,1:T(8,128)(2,1)} %bitcast.109), kind=kOutput, calls=%fused_computation.26 | convolution fusion | flops 8390656 | bytes 2117632 | tf_op jit(solution)/shard_map/dot_general | solution.py:113
  62.4 2.0 %fusion.18 = f32[4,2048]{1,0:T(4,128)S(1)} fusion(bf16[64,8,16,128]{3,2,1,0:T(8,128)(2,1)} %bitcast.108, bf16[4,2048]{1,0:T(4,128)(2,1)S(1)} %fusion.47, s32[]{:T(128)S(6)} %select_n.11), kind=kOutput, calls=%fused_computation.18 | convolution fusion | flops 8388608 | bytes 2134020 | tf_op jit(solution)/shard_map/dot_general | solution.py:80
  65.0 19.8 %all-reduce.2 = (bf16[4,2048]{1,0:T(4,128)(2,1)S(1)}, f32[4,64]{1,0:T(4,128)S(1)}) all-reduce(f32[4,2048]{1,0:T(4,128)S(1)} %fusion.18, f32[4,64]{1,0:T(4,128)S(1)} %fusion.69), channel_id=4, replica_groups=mesh['dp'=4,'kv'=4,'tp'=2] {'kv'}, use_global_device_ids=true, to_apply=%region_6.7.clone | all-reduce | flops 8448 | bytes 51200
  84.8 0.7 fusion.60
  85.7 0.7 reshape.217
  86.3 3.2 %all-to-all-start.1 = ((bf16[4,2,256]{2,1,0:T(2,128)(2,1)}), bf16[4,2,256]{2,1,0:T(2,128)(2,1)S(1)}, u32[]{:S(2)}, u32[]{:S(2)}) async-start(bf16[4,2,256]{2,1,0:T(2,128)(2,1)} %reshape.217), calls=%async_computation.1 | async-start | bytes 8192 | tf_op jit(solution)/shard_map/all_to_all | solution.py:119
  90.5 4.7 %all-to-all-done.1 = bf16[4,2,256]{2,1,0:T(2,128)(2,1)S(1)} async-done(((bf16[4,2,256]{2,1,0:T(2,128)(2,1)}), bf16[4,2,256]{2,1,0:T(2,128)(2,1)S(1)}, u32[]{:S(2)}, u32[]{:S(2)}) %all-to-all-start.1) | async-done | bytes 4128 | tf_op jit(solution)/shard_map/all_to_all | solution.py:119
  95.5 1.9 %fusion.33 = f32[64,1,32]{2,1,0:T(1,128)S(1)} fusion(f32[64,128,1]{1,2,0:T(1,128)S(1)} %bitcast.110, f32[1,64,32,128]{3,2,1,0:T(8,128)S(1)} %copy-done.1, f32[64,128]{1,0:T(8,128)S(1)} %broadcast_bitcast_fusion, f32[64,32]{1,0:T(8,128)S(1)} %copy.28, f32[64]{0:T(128)S(1)} %get-tuple-element.7), kind=kOutput, calls=%fused_computation.28 | convolution fusion | flops 3932160 | bytes 1130752 | tf_op jit(solution)/shard_map/shpn,shn->shp/dot_general | solution.py:71
  97.5 13.1 %all-gather.1 = bf16[4,64,32]{1,2,0:T(8,128)(2,1)S(1)} all-gather(bf16[1,64,32]{1,2,0:T(8,128)(2,1)S(1)} %fusion.64), channel_id=2, replica_groups=mesh['dp'=4,'kv'=4,'tp'=2] {'kv'}, dimensions={0}, use_global_device_ids=true | all-gather | bytes 20480 | tf_op jit(solution)/shard_map/all_gather | solution.py:140
  110.7 2.0 %convolution_bitcast_fusion = f32[4,512]{1,0:T(4,128)S(1)} fusion(bf16[4,64,32]{2,0,1:T(4,128)(2,1)S(1)} %copy.35, bf16[64,32,512]{2,1,0:T(8,128)(2,1)} %param.35), kind=kOutput, calls=%fused_computation.25 | convolution fusion | flops 8388608 | bytes 2121728 | tf_op jit(solution)/shard_map/dot_general | solution.py:141
  112.7 2.5 %psum.37 = f32[4,512]{1,0:T(4,128)S(1)} all-reduce(f32[4,512]{1,0:T(4,128)S(1)} %convolution_bitcast_fusion), channel_id=1, replica_groups=mesh['dp'=4,'kv'=4,'tp'=2] {'tp'}, use_global_device_ids=true, to_apply=%region_8.9 | all-reduce | flops 2048 | bytes 16384 | tf_op jit(solution)/shard_map/psum | solution.py:190
  115.2 13.2 %all_gather.15 = bf16[4,2048]{1,0:T(4,128)(2,1)S(1)} all-gather(bf16[4,512]{1,0:T(4,128)(2,1)S(1)} %add_convert_fusion), channel_id=1, replica_groups=mesh['dp'=4,'kv'=4,'tp'=2] {'kv'}, dimensions={1}, use_global_device_ids=true | all-gather | bytes 20480 | tf_op jit(solution)/shard_map/all_gather | solution.py:191
  128.6 2.7 %fusion.4 = f32[4,704]{1,0:T(4,128)S(1)} fusion(bf16[2,2048,704]{1,2,0:T(8,128)(2,1)} %param.20, f32[2048]{0:T(1024)S(1)} %bitcast.111, f32[4]{0:T(128)S(1)} %add_rsqrt_fusion, bf16[4,2048]{1,0:T(4,128)(2,1)S(1)} %all_gather.15), kind=kOutput, calls=%fused_computation.4 | convolution fusion | flops 11567104 | bytes 2919440 | tf_op jit(solution)/shard_map/dot_general | solution.py:23
  131.2 4.4 %fusion = f32[4,2048]{1,0:T(4,128)S(1)} fusion(bf16[2,704,2048]{2,1,0:T(8,128)(2,1)} %param.22, bf16[2,2048,704]{1,2,0:T(8,128)(2,1)} %param.21, f32[4,704]{1,0:T(4,128)S(1)} %fusion.4, f32[2048]{0:T(1024)S(1)} %bitcast.112, f32[4]{0:T(128)S(1)} %add_rsqrt_fusion, bf16[4,2048]{1,0:T(4,128)(2,1)S(1)} %all_gather.15), kind=kOutput, calls=%fused_computation | convolution fusion | flops 23118336 | bytes 5835792 | tf_op jit(solution)/shard_map/dot_general | solution.py:26
  135.6 3.4 %psum.38 = f32[4,2048]{1,0:T(4,128)S(1)} all-reduce(f32[4,2048]{1,0:T(4,128)S(1)} %fusion), channel_id=1, replica_groups=mesh['dp'=4,'kv'=4,'tp'=2] {'tp'}, use_global_device_ids=true, to_apply=%region_10.11 | all-reduce | flops 8192 | bytes 65536 | tf_op jit(solution)/shard_map/psum | solution.py:12
  139.0 16.2 %psum.39 = f32[4,2048]{1,0:T(4,128)S(1)} all-reduce(f32[4,2048]{1,0:T(4,128)S(1)} %psum.38), channel_id=1, replica_groups=mesh['dp'=4,'kv'=4,'tp'=2] {'kv'}, use_global_device_ids=true, to_apply=%region_11.12 | all-reduce | flops 8192 | bytes 65536 | tf_op jit(solution)/shard_map/psum | solution.py:12
  (56 shorter events, 4.1 us)
Async XLA Ops:
  0.0 55.2 %copy-start = (bf16[2048,16,32]{0,2,1:T(8,128)(2,1)S(1)}, bf16[2048,16,32]{0,2,1:T(8,128)(2,1)}, u32[]{:S(2)}) copy-start(bf16[2048,16,32]{0,2,1:T(8,128)(2,1)} %param.23) | copy-start | bytes 6291460
  34.8 27.4 %copy-start.2 = (bf16[512,64]{0,1:T(8,128)(2,1)S(1)}, bf16[512,64]{0,1:T(8,128)(2,1)}, u32[]{:S(2)}) copy-start(bf16[512,64]{0,1:T(8,128)(2,1)} %param.26) | copy-start | bytes 196612
  55.2 9.1 %copy-start.10 = (u32[32]{0:T(128)S(1)}, u32[32]{0:T(128)}, u32[]{:S(2)}) copy-start(u32[32]{0:T(128)} %constant.45) | copy-start | bytes 388
  55.3 30.2 %copy-start.5 = (bf16[4,2,8,128]{3,2,1,0:T(8,128)(2,1)S(1)}, bf16[4,2,8,128]{3,2,1,0:T(8,128)(2,1)}, u32[]{:S(2)}) copy-start(bf16[4,2,8,128]{3,2,1,0:T(8,128)(2,1)} %param.31) | copy-start | bytes 49156
  55.3 30.2 %copy-start.6 = (bf16[1,3,2,8,128]{4,3,2,1,0:T(8,128)(2,1)S(1)}, bf16[1,3,2,8,128]{4,3,2,1,0:T(8,128)(2,1)}, u32[]{:S(2)}) copy-start(bf16[1,3,2,8,128]{4,3,2,1,0:T(8,128)(2,1)} %param.33) | copy-start | bytes 36868
  55.3 34.3 %copy-start.8 = (f32[64]{0:T(128)S(1)}, f32[64]{0:T(128)}, u32[]{:S(2)}) copy-start(f32[64]{0:T(128)} %param.28) | copy-start | bytes 772
  55.3 34.3 %copy-start.9 = (f32[64]{0:T(128)S(1)}, f32[64]{0:T(128)}, u32[]{:S(2)}) copy-start(f32[64]{0:T(128)} %param.27) | copy-start | bytes 772
  55.9 39.4 %copy-start.3 = (bf16[4,64,32]{1,2,0:T(8,128)(2,1)S(1)}, bf16[4,64,32]{1,2,0:T(8,128)(2,1)}, u32[]{:S(2)}) copy-start(bf16[4,64,32]{1,2,0:T(8,128)(2,1)} %param.30) | copy-start | bytes 49156
  55.9 39.4 %copy-start.4 = (bf16[1,3,64,32]{2,3,1,0:T(8,128)(2,1)S(1)}, bf16[1,3,64,32]{2,3,1,0:T(8,128)(2,1)}, u32[]{:S(2)}) copy-start(bf16[1,3,64,32]{2,3,1,0:T(8,128)(2,1)} %param.32) | copy-start | bytes 36868
  56.0 39.5 %copy-start.1 = (f32[1,64,32,128]{3,2,1,0:T(8,128)S(1)}, f32[1,64,32,128]{3,2,1,0:T(8,128)}, u32[]{:S(2)}) copy-start(f32[1,64,32,128]{3,2,1,0:T(8,128)} %param.34) | copy-start | bytes 3145732
  56.7 29.6 %all-to-all-start = ((bf16[4,2,256]{2,1,0:T(2,128)(2,1)}), bf16[4,2,256]{2,1,0:T(2,128)(2,1)S(1)}, u32[]{:S(2)}, u32[]{:S(2)}) async-start(bf16[4,2,256]{2,1,0:T(2,128)(2,1)} %reshape.219), calls=%async_computation | async-start | bytes 8192 | tf_op jit(solution)/shard_map/all_to_all | solution.py:118
  60.0 37.4 %copy-start.7 = (f32[64]{0:T(128)S(1)}, f32[64]{0:T(128)}, u32[]{:S(2)}) copy-start(f32[64]{0:T(128)} %param.29) | copy-start | bytes 772
  86.3 8.8 %all-to-all-start.1 = ((bf16[4,2,256]{2,1,0:T(2,128)(2,1)}), bf16[4,2,256]{2,1,0:T(2,128)(2,1)S(1)}, u32[]{:S(2)}, u32[]{:S(2)}) async-start(bf16[4,2,256]{2,1,0:T(2,128)(2,1)} %reshape.217), calls=%async_computation.1 | async-start | bytes 8192 | tf_op jit(solution)/shard_map/all_to_all | solution.py:119
